TPU v7x, 32 devices: a whole 2x2x4 slice. The times are simulated.
32 devices in a mesh: rep: 2 (over y), fs: 4 (over z), tp: 4 (over x, core).
Axes of the slice: x: 2, y: 2, z: 4, core: 2. Of those that a mesh axis runs over, the one named last changes fastest.
Arguments:
- stream: bfloat16 [2048, 1536], P(('rep', 'fs')), may hold values from -6 to 6
- mix_pre_gain: float32 [1536], replicated, may hold values from 0.1 to 1.9
- w_outer_gate: bfloat16 [1536, 768], P('fs', 'tp'), may hold values from -0.15625 to 0.15625
- w_inner_gate: bfloat16 [1536, 768], P('fs', 'tp'), may hold values from -0.15625 to 0.15625
- w_value: bfloat16 [1536, 768], P('fs', 'tp'), may hold values from -0.15625 to 0.15625
- mix_taps: float32 [3, 768], P(None, 'tp'), may hold values from -3 to 3
- w_mix_out: bfloat16 [768, 1536], P('tp', 'fs'), may hold values from -0.3125 to 0.3125
- mix_post_gain: float32 [1536], replicated, may hold values from 0.1 to 1.9
- ffn_pre_gain: float32 [1536], replicated, may hold values from 0.1 to 1.9
- w_linear: bfloat16 [1536, 4224], P('fs', 'tp'), may hold values from -0.15625 to 0.15625
- w_gated: bfloat16 [1536, 4224], P('fs', 'tp'), may hold values from -0.15625 to 0.15625
- ffn_taps: float32 [3, 4224], P(None, 'tp'), may hold values from -3 to 3
- ffn_bias: float32 [4224], P('tp'), may hold values from -3 to 3
- w_down: bfloat16 [4224, 1536], P('tp', 'fs'), may hold values from -0.125 to 0.125
- ffn_post_gain: float32 [1536], replicated, may hold values from 0.1 to 1.9
Outputs:
- result: bfloat16 [2048, 1536], P(('rep', 'fs'))
All inputs are finite; a program needn't handle non-finite values.
Results may differ from a plain program's by a relative error of at most 0.023.
Values may be sent and summed in bfloat16 or wider, within the bound.
A program may use at most 64 MiB of HBM per device.

v0:
```python
import jax
import jax.numpy as jnp
from jax import lax
from jax.sharding import PartitionSpec as P

SEQ_LEN = 128
EPS = 1e-06


def norm_scale(values, gain):
    return values * lax.rsqrt(jnp.mean(values * values, axis=-1, keepdims=True) + EPS) * gain


def conv_three(values, taps):
    height, breadth = values.shape
    grouped = values.reshape(height // SEQ_LEN, SEQ_LEN, breadth)
    padded = jnp.pad(grouped, ((0, 0), (1, 1), (0, 0)))
    mixed = taps[0] * padded[:, :-2] + taps[1] * padded[:, 1:-1] + taps[2] * padded[:, 2:]
    return mixed.reshape(height, breadth)


def settle(partial_value, resid, post_gain):
    branch = lax.psum(partial_value.astype(jnp.bfloat16), "tp")
    return (resid + norm_scale(branch.astype(jnp.float32), post_gain)).astype(jnp.bfloat16)


def on_device(
    stream,
    mix_pre_gain,
    w_outer_gate,
    w_inner_gate,
    w_value,
    mix_taps,
    w_mix_out,
    mix_post_gain,
    ffn_pre_gain,
    w_linear,
    w_gated,
    ffn_taps,
    ffn_bias,
    w_down,
    ffn_post_gain,
):
    resid = stream.astype(jnp.float32)
    normed = norm_scale(resid, mix_pre_gain).astype(jnp.bfloat16)
    full_outer, full_inner, full_value = (
        lax.all_gather(w_outer_gate, "fs", axis=0, tiled=True),
        lax.all_gather(w_inner_gate, "fs", axis=0, tiled=True),
        lax.all_gather(w_value, "fs", axis=0, tiled=True),
    )
    outer = jnp.dot(normed, full_outer, preferred_element_type=jnp.float32)
    inner = jnp.dot(normed, full_inner, preferred_element_type=jnp.float32)
    value = jnp.dot(normed, full_value, preferred_element_type=jnp.float32)
    outer = outer.astype(jnp.bfloat16)
    inner = inner.astype(jnp.bfloat16)
    value = value.astype(jnp.bfloat16)
    product = inner.astype(jnp.float32) * value.astype(jnp.float32)
    mixed = (outer.astype(jnp.float32) * conv_three(product, mix_taps)).astype(jnp.bfloat16)
    full_mix_out = lax.all_gather(w_mix_out, "fs", axis=1, tiled=True)
    partial_value = jnp.dot(mixed, full_mix_out, preferred_element_type=jnp.float32)
    middle = settle(partial_value, resid, mix_post_gain)
    middle_f = middle.astype(jnp.float32)
    normed_two = norm_scale(middle_f, ffn_pre_gain).astype(jnp.bfloat16)
    full_linear, full_gated = (
        lax.all_gather(w_linear, "fs", axis=0, tiled=True),
        lax.all_gather(w_gated, "fs", axis=0, tiled=True),
    )
    linear = jnp.dot(normed_two, full_linear, preferred_element_type=jnp.float32)
    gated = jnp.dot(normed_two, full_gated, preferred_element_type=jnp.float32)
    linear = linear.astype(jnp.bfloat16)
    gated = gated.astype(jnp.bfloat16)
    activated = jax.nn.gelu(
        conv_three(gated.astype(jnp.float32), ffn_taps) + ffn_bias, approximate=True
    )
    hidden = (activated * linear.astype(jnp.float32)).astype(jnp.bfloat16)
    full_down = lax.all_gather(w_down, "fs", axis=1, tiled=True)
    partial_two = jnp.dot(hidden, full_down, preferred_element_type=jnp.float32)
    return settle(partial_two, middle_f, ffn_post_gain)


def solution(mesh):
    in_specs = (
        P(("rep", "fs"), None),
        P(),
        P("fs", "tp"),
        P("fs", "tp"),
        P("fs", "tp"),
        P(None, "tp"),
        P("tp", "fs"),
        P(),
        P(),
        P("fs", "tp"),
        P("fs", "tp"),
        P(None, "tp"),
        P("tp"),
        P("tp", "fs"),
        P(),
    )
    out_specs = P(("rep", "fs"), None)
    return jax.shard_map(
        on_device, mesh=mesh, in_specs=in_specs, out_specs=out_specs, check_vma=False
    )
```

profile of v0, /device:TPU:0, one launch (start us, length us, event | category | flops | bytes accessed | tf_op | source)
XLA Modules:
  0.0 331.4 jit_solution(645357725762932306)
XLA Ops:
  7.4 1.5 fusion.8
  8.8 18.7 %all_gather.22 = bf16[1536,192]{0,1:T(8,128)(2,1)S(1)} all-gather(bf16[384,192]{0,1:T(8,128)(2,1)} %param.18), channel_id=1, replica_groups=mesh['rep'=2,'fs'=4,'tp'=4] {'fs'}, dimensions={0}, use_global_device_ids=true | all-gather | bytes 737280 | tf_op jit(solution)/shard_map/all_gather | solution.py:48
  27.5 16.1 %all_gather.23 = bf16[1536,192]{0,1:T(8,128)(2,1)S(1)} all-gather(bf16[384,192]{0,1:T(8,128)(2,1)S(1)} %copy-done.1), channel_id=1, replica_groups=mesh['rep'=2,'fs'=4,'tp'=4] {'fs'}, dimensions={0}, use_global_device_ids=true | all-gather | bytes 737280 | tf_op jit(solution)/shard_map/all_gather | solution.py:49
  44.2 0.5 fusion.17
  45.1 16.4 %all_gather.21 = bf16[1536,192]{0,1:T(8,128)(2,1)S(1)} all-gather(bf16[384,192]{0,1:T(8,128)(2,1)S(1)} %copy-done.2), channel_id=1, replica_groups=mesh['rep'=2,'fs'=4,'tp'=4] {'fs'}, dimensions={0}, use_global_device_ids=true | all-gather | bytes 737280 | tf_op jit(solution)/shard_map/all_gather | solution.py:47
  61.5 15.5 %all_gather.24 = bf16[192,1536]{1,0:T(8,128)(2,1)S(1)} all-gather(bf16[192,384]{1,0:T(8,128)(2,1)S(1)} %copy-done.3), channel_id=1, replica_groups=mesh['rep'=2,'fs'=4,'tp'=4] {'fs'}, dimensions={1}, use_global_device_ids=true | all-gather | bytes 737280 | tf_op jit(solution)/shard_map/all_gather | solution.py:59
  77.0 1.2 fusion.43
  78.2 2.1 convolution_convert_fusion.3
  80.4 0.5 all-gather.4.cloned.1.call-update
  81.0 0.5 all-gather.6.cloned.1.call-update
  81.6 0.5 all-gather.8.cloned.1.call-update
  82.2 34.8 %all-reduce.5.cloned.1.call-done = bf16[256,1536]{1,0:T(8,128)(2,1)} async-done(((bf16[256,1536]{1,0:T(8,128)(2,1)}), bf16[256,1536]{1,0:T(8,128)(2,1)}) %all-reduce.5.cloned.1.call-update) | async-done | bytes 786448 | tf_op jit(solution)/shard_map/psum | solution.py:23
  117.0 1.4 fusion.4
  118.4 1.7 fusion.12
  120.1 28.7 %all-gather.4.cloned.1.call-done = bf16[1536,1056]{0,1:T(8,128)(2,1)} async-done(((bf16[384,1056]{0,1:T(8,128)(2,1)}), bf16[1536,1056]{0,1:T(8,128)(2,1)}) %all-gather.4.cloned.1.call-update) | async-done | bytes 3244048 | tf_op jit(solution)/shard_map/all_gather | solution.py:66
  148.7 4.0 %fusion.2 = f32[256,1056]{0,1:T(8,128)} fusion(bf16[1536,1056]{0,1:T(8,128)(2,1)} %all-gather.4.cloned.1.call-done, bf16[256,1536]{1,0:T(8,128)(2,1)S(1)} %get-tuple-element.9, f32[1536]{0:T(1024)S(1)} %copy-done.9, f32[256]{0:T(256)S(1)} %add_rsqrt_fusion.1), kind=kOutput, calls=%fused_computation.4 | convolution fusion | flops 832585728 | bytes 5118976 | tf_op jit(solution)/shard_map/dot_general | solution.py:69
  152.8 1.8 reshape.64
  154.6 7.3 %fusion.31 = f32[2,128,1056]{1,0,2:T(2,128)} fusion(f32[2,128,1056]{1,0,2:T(2,128)S(1)} %reshape.64, f32[1056]{0:T(1024)S(1)} %get-tuple-element.6, f32[1056]{0:T(1024)S(1)} %get-tuple-element.7, f32[1056]{0:T(1024)S(1)} %get-tuple-element.5), kind=kLoop, calls=%fused_computation.51 | loop fusion | flops 1351680 | bytes 2175360 | tf_op jit(solution)/shard_map/add | solution.py:18
  162.0 51.6 %all-gather.6.cloned.1.call-done = bf16[1536,1056]{0,1:T(8,128)(2,1)} async-done(((bf16[384,1056]{0,1:T(8,128)(2,1)}), bf16[1536,1056]{0,1:T(8,128)(2,1)}) %all-gather.6.cloned.1.call-update) | async-done | bytes 3244048 | tf_op jit(solution)/shard_map/all_gather | solution.py:65
  213.5 64.8 %all-gather.8.cloned.1.call-done = bf16[1056,1536]{1,0:T(8,128)(2,1)} async-done(((bf16[1056,384]{1,0:T(8,128)(2,1)}), bf16[1056,1536]{1,0:T(8,128)(2,1)}) %all-gather.8.cloned.1.call-update) | async-done | bytes 3244048 | tf_op jit(solution)/shard_map/all_gather | solution.py:76
  278.3 7.9 %convolution_convert_fusion.2 = bf16[256,1536]{1,0:T(8,128)(2,1)} fusion(bf16[1056,1536]{1,0:T(8,128)(2,1)} %all-gather.8.cloned.1.call-done, bf16[1536,1056]{0,1:T(8,128)(2,1)} %all-gather.6.cloned.1.call-done, f32[132,8,2,128]{3,2,1,0:T(2,128)} %bitcast.31, f32[1056]{0:T(1024)S(1)} %copy-done.10, bf16[256,1536]{1,0:T(8,128)(2,1)S(1)} %get-tuple-element.9, ...), kind=kOutput, calls=%fused_computation.6 | convolution fusion | flops 1666424832 | bytes 9153664 | tf_op jit(solution)/shard_map/dot_general | solution.py:77
  286.3 33.8 %all-reduce.7.cloned.1.call-done = bf16[256,1536]{1,0:T(8,128)(2,1)} async-done(((bf16[256,1536]{1,0:T(8,128)(2,1)}), bf16[256,1536]{1,0:T(8,128)(2,1)}) %all-reduce.7.cloned.1.call-update) | async-done | bytes 786448 | tf_op jit(solution)/shard_map/psum | solution.py:23
  320.1 1.4 fusion.6
  321.5 2.4 fusion.15
  (37 shorter events, 1.2 us)
Async XLA Ops:
  7.4 36.3 %copy-start = (bf16[256,1536]{1,0:T(8,128)(2,1)S(1)}, bf16[256,1536]{1,0:T(8,128)(2,1)}, u32[]{:S(2)}) copy-start(bf16[256,1536]{1,0:T(8,128)(2,1)} %param.15) | copy-start | bytes 2359300
  7.4 20.2 %copy-start.1 = (bf16[384,192]{0,1:T(8,128)(2,1)S(1)}, bf16[384,192]{0,1:T(8,128)(2,1)}, u32[]{:S(2)}) copy-start(bf16[384,192]{0,1:T(8,128)(2,1)} %param.19) | copy-start | bytes 442372
  7.4 36.3 %copy-start.8 = (f32[1536]{0:T(1024)S(1)}, f32[1536]{0:T(1024)}, u32[]{:S(2)}) copy-start(f32[1536]{0:T(1024)} %param.16) | copy-start | bytes 18436
  7.4 109.6 %all-reduce.5.cloned.1.call-start = ((), (), s32[]{:S(2)}) async-start(), calls=%async_computation | async-start | bytes 1572864 | tf_op jit(solution)/shard_map/psum | solution.py:23
  44.2 0.7 copy-start.7
  44.2 0.9 copy-start.2
  44.2 17.3 %copy-start.3 = (bf16[192,384]{1,0:T(8,128)(2,1)S(1)}, bf16[192,384]{1,0:T(8,128)(2,1)}, u32[]{:S(2)}) copy-start(bf16[192,384]{1,0:T(8,128)(2,1)} %param.21) | copy-start | bytes 442372
  80.3 1.8 copy-start.4
  80.4 38.0 %copy-start.5 = (f32[1536]{0:T(1024)S(1)}, f32[1536]{0:T(1024)}, u32[]{:S(2)}) copy-start(f32[1536]{0:T(1024)} %param.22) | copy-start | bytes 18436
  80.4 68.4 %all-gather.4.cloned.1.call-start = ((), (), s32[]{:S(2)}) async-start(), calls=%async_computation.1 | async-start | bytes 4055040 | tf_op jit(solution)/shard_map/all_gather | solution.py:66
  80.9 132.6 %all-gather.6.cloned.1.call-start = ((), (), s32[]{:S(2)}) async-start(), calls=%async_computation.2 | async-start | bytes 4055040 | tf_op jit(solution)/shard_map/all_gather | solution.py:65
  81.5 196.8 %all-gather.8.cloned.1.call-start = ((), (), s32[]{:S(2)}) async-start(), calls=%async_computation.3 | async-start | bytes 4055040 | tf_op jit(solution)/shard_map/all_gather | solution.py:76
  82.1 238.0 %all-reduce.7.cloned.1.call-start = ((), (), s32[]{:S(2)}) async-start(), calls=%async_computation.4 | async-start | bytes 1572864 | tf_op jit(solution)/shard_map/psum | solution.py:23
  82.2 66.5 %copy-start.9 = (f32[1536]{0:T(1024)S(1)}, f32[1536]{0:T(1024)}, u32[]{:S(2)}) copy-start(f32[1536]{0:T(1024)} %param.23) | copy-start | bytes 18436
  154.6 123.7 %copy-start.10 = (f32[1056]{0:T(1024)S(1)}, f32[1056]{0:T(1024)}, u32[]{:S(2)}) copy-start(f32[1056]{0:T(1024)} %param.27) | copy-start | bytes 12676
  286.3 35.2 %copy-start.6 = (f32[1536]{0:T(1024)S(1)}, f32[1536]{0:T(1024)}, u32[]{:S(2)}) copy-start(f32[1536]{0:T(1024)} %param.29) | copy-start | bytes 18436
Sparse Core Ops, SparseCore 0:
  80.5 36.4 all-reduce.4
  286.4 33.6 all-reduce.6
Sparse Core Ops, SparseCore 1:
  82.4 66.2 all-gather.3
  150.2 63.3 all-gather.5
  215.0 63.3 all-gather.7
where the time goes:
time: 332 us; the launch traced here: 331 us
  waiting for transfers between devices  215 us (65%)
  blocking collectives  66.7 us (20%)
  other arithmetic  16.8 us (5%)
  between operations  15.2 us (5%)
  matrix products  15.1 us (5%)
    psum x2, waiting for transfers between devices, settle(): branch = lax.psum(partial_value.astype(jnp.bfloat16), 'tp')  68.6 us
    all_gather x1, waiting for transfers between devices, on_device(): full_down = lax.all_gather(w_down, 'fs', axis=1, tiled=True)  64.8 us
    all_gather x1, waiting for transfers between devices, on_device(): lax.all_gather(w_linear, 'fs', axis=0, tiled=True)  51.6 us
    all_gather x1, waiting for transfers between devices, on_device(): lax.all_gather(w_gated, 'fs', axis=0, tiled=True)  28.7 us
    all_gather x1, blocking collectives, on_device(): lax.all_gather(w_inner_gate, 'fs', axis=0, tiled=True)  18.7 us
    all_gather x1, blocking collectives, on_device(): lax.all_gather(w_outer_gate, 'fs', axis=0, tiled=True)  16.4 us
    all_gather x1, blocking collectives, on_device(): lax.all_gather(w_value, 'fs', axis=0, tiled=True)  16.1 us
    all_gather x1, blocking collectives, on_device(): full_mix_out = lax.all_gather(w_mix_out, 'fs', axis=1, tiled=True)  15.5 us
  transfers between devices with their start and end apart: 5, of which 5 were waited for; matrix products, arithmetic and copies ran while one was open for 5% of the time, Pallas kernels for 0%

commit v1 on v0

--- a/solution.py
+++ b/solution.py
@@ -73,7 +73,12 @@
         conv_three(gated.astype(jnp.float32), ffn_taps) + ffn_bias, approximate=True
     )
     hidden = (activated * linear.astype(jnp.float32)).astype(jnp.bfloat16)
-    full_down = lax.all_gather(w_down, "fs", axis=1, tiled=True)
+    ring = [w_down]
+    for hop in range(3):
+        ring.append(lax.ppermute(ring[-1], "fs", [(dev, (dev + 1) % 4) for dev in range(4)]))
+    full_down = jnp.roll(
+        jnp.concatenate(ring[::-1], axis=1), (lax.axis_index("fs") + 1) * ring[0].shape[1], axis=1
+    )
     partial_two = jnp.dot(hidden, full_down, preferred_element_type=jnp.float32)
     return settle(partial_two, middle_f, ffn_post_gain)
 

time: 332 us -> 294 us (0.89)
  waiting for transfers between devices: 215 us -> 139 us
  starting transfers between devices: 0.17 us -> 31.1 us
  local copies, waits for them, and re-layouts: 2.28 us -> 9.73 us
    ppermute x0 -> x3, waiting for transfers between devices: none -> 66.6 us  [on_device(): lax.ppermute(ring[-1], 'fs', [(dev, (dev + 1) % 4) for dev in range(4)])]
    all_gather x1 -> x0, waiting for transfers between devices: 64.8 us -> none  [on_device(): full_down = lax.all_gather(w_down, 'fs', axis=1, tiled=True)]
    psum x2, waiting for transfers between devices: 68.6 us -> 33.8 us  [settle(): branch = lax.psum(partial_value.astype(jnp.bfloat16), 'tp')]
    ppermute x0 -> x3, starting transfers between devices: none -> 31 us  [on_device(): lax.ppermute(ring[-1], 'fs', [(dev, (dev + 1) % 4) for dev in range(4)])]
    all_gather x1, waiting for transfers between devices: 28.7 us -> 0.01 us  [on_device(): lax.all_gather(w_gated, 'fs', axis=0, tiled=True)]
    all_gather x1, waiting for transfers between devices: 51.6 us -> 38.4 us  [on_device(): lax.all_gather(w_linear, 'fs', axis=0, tiled=True)]
    unnamed x22 -> x31, local copies, waits for them, and re-layouts: 0.32 us -> 7.97 us
    all_gather x1, blocking collectives: 15.5 us -> 18.8 us  [on_device(): full_mix_out = lax.all_gather(w_mix_out, 'fs', axis=1, tiled=True)]
  transfers between devices with their start and end apart: 5 -> 7, of which waited for: 5 -> 5; matrix products, arithmetic and copies ran while one was open for 5% -> 8% of each run, Pallas kernels for 0% -> 0%
where the time goes in v1:
time: 294 us; the launch traced here: 293 us
  waiting for transfers between devices  139 us (47%)
  blocking collectives  68.3 us (23%)
  starting transfers between devices  31.1 us (11%)
  other arithmetic  15.7 us (5%)
  between operations  15 us (5%)
  matrix products  14 us (5%)
  local copies, waits for them, and re-layouts  9.73 us (3%)
    ppermute x3, waiting for transfers between devices, on_device(): lax.ppermute(ring[-1], 'fs', [(dev, (dev + 1) % 4) for dev in range(4)])  66.6 us
    all_gather x1, waiting for transfers between devices, on_device(): lax.all_gather(w_linear, 'fs', axis=0, tiled=True)  38.4 us
    psum x2, waiting for transfers between devices, settle(): branch = lax.psum(partial_value.astype(jnp.bfloat16), 'tp')  33.8 us
    ppermute x3, starting transfers between devices, on_device(): lax.ppermute(ring[-1], 'fs', [(dev, (dev + 1) % 4) for dev in range(4)])  31 us
    all_gather x1, blocking collectives, on_device(): full_mix_out = lax.all_gather(w_mix_out, 'fs', axis=1, tiled=True)  18.8 us
    all_gather x1, blocking collectives, on_device(): lax.all_gather(w_outer_gate, 'fs', axis=0, tiled=True)  17.3 us
    all_gather x1, blocking collectives, on_device(): lax.all_gather(w_value, 'fs', axis=0, tiled=True)  16.1 us
    all_gather x1, blocking collectives, on_device(): lax.all_gather(w_inner_gate, 'fs', axis=0, tiled=True)  16 us
  transfers between devices with their start and end apart: 7, of which 5 were waited for; matrix products, arithmetic and copies ran while one was open for 8% of the time, Pallas kernels for 0%

profile of v1, /device:TPU:0, one launch (start us, length us, event | category | flops | bytes accessed | tf_op | source)
XLA Modules:
  0.0 293.1 jit_solution(7228122063508324441)
XLA Ops:
  7.4 18.8 %all_gather.21 = bf16[192,1536]{1,0:T(8,128)(2,1)S(1)} all-gather(bf16[192,384]{1,0:T(8,128)(2,1)} %param.21), channel_id=1, replica_groups=mesh['rep'=2,'fs'=4,'tp'=4] {'fs'}, dimensions={1}, use_global_device_ids=true | all-gather | bytes 737280 | tf_op jit(solution)/shard_map/all_gather | solution.py:59
  26.2 17.3 %all_gather.18 = bf16[1536,192]{0,1:T(8,128)(2,1)S(1)} all-gather(bf16[384,192]{0,1:T(8,128)(2,1)} %param.17), channel_id=1, replica_groups=mesh['rep'=2,'fs'=4,'tp'=4] {'fs'}, dimensions={0}, use_global_device_ids=true | all-gather | bytes 737280 | tf_op jit(solution)/shard_map/all_gather | solution.py:47
  43.5 16.0 %all_gather.19 = bf16[1536,192]{0,1:T(8,128)(2,1)S(1)} all-gather(bf16[384,192]{0,1:T(8,128)(2,1)S(1)} %copy-done.3), channel_id=1, replica_groups=mesh['rep'=2,'fs'=4,'tp'=4] {'fs'}, dimensions={0}, use_global_device_ids=true | all-gather | bytes 737280 | tf_op jit(solution)/shard_map/all_gather | solution.py:48
  59.8 16.1 %all_gather.20 = bf16[1536,192]{0,1:T(8,128)(2,1)S(1)} all-gather(bf16[384,192]{0,1:T(8,128)(2,1)S(1)} %copy-done.4), channel_id=1, replica_groups=mesh['rep'=2,'fs'=4,'tp'=4] {'fs'}, dimensions={0}, use_global_device_ids=true | all-gather | bytes 737280 | tf_op jit(solution)/shard_map/all_gather | solution.py:49
  77.1 1.2 fusion.48
  78.3 2.1 convolution_convert_fusion.2
  81.6 8.4 %collective-permute-start = (bf16[1056,384]{1,0:T(8,128)(2,1)S(1)}, bf16[1056,384]{1,0:T(8,128)(2,1)S(1)}, u32[]{:S(2)}, u32[]{:S(2)}) collective-permute-start(bf16[1056,384]{1,0:T(8,128)(2,1)S(1)} %copy-done), channel_id=1, source_target_pairs={{0,4},{4,8},{8,12},{12,0},{1,5},{5,9},{9,13},{13,1},{2,6},{6,10},{... | collective-permute-start | bytes 2433032 | tf_op jit(solution)/shard_map/ppermute | solution.py:78
  90.1 19.6 %collective-permute-done = bf16[1056,384]{1,0:T(8,128)(2,1)S(1)} collective-permute-done((bf16[1056,384]{1,0:T(8,128)(2,1)S(1)}, bf16[1056,384]{1,0:T(8,128)(2,1)S(1)}, u32[]{:S(2)}, u32[]{:S(2)}) %collective-permute-start) | collective-permute-done | bytes 811040 | tf_op jit(solution)/shard_map/ppermute | solution.py:78
  109.7 5.5 %collective-permute-start.1 = (bf16[1056,384]{1,0:T(8,128)(2,1)S(1)}, bf16[1056,384]{1,0:T(8,128)(2,1)S(1)}, u32[]{:S(2)}, u32[]{:S(2)}) collective-permute-start(bf16[1056,384]{1,0:T(8,128)(2,1)S(1)} %collective-permute-done), channel_id=1, source_target_pairs={{0,4},{4,8},{8,12},{12,0},{1,5},{5,9},{9,13},{13,1},{2,6},{6,10},{... | collective-permute-start | bytes 2433032 | tf_op jit(solution)/shard_map/ppermute | solution.py:78
  115.2 36.1 %collective-permute-done.1 = bf16[1056,384]{1,0:T(8,128)(2,1)S(1)} collective-permute-done((bf16[1056,384]{1,0:T(8,128)(2,1)S(1)}, bf16[1056,384]{1,0:T(8,128)(2,1)S(1)}, u32[]{:S(2)}, u32[]{:S(2)}) %collective-permute-start.1) | collective-permute-done | bytes 811040 | tf_op jit(solution)/shard_map/ppermute | solution.py:78
  151.3 17.1 %collective-permute-start.2 = (bf16[1056,384]{1,0:T(8,128)(2,1)S(1)}, bf16[1056,384]{1,0:T(8,128)(2,1)S(1)}, u32[]{:S(2)}, u32[]{:S(2)}) collective-permute-start(bf16[1056,384]{1,0:T(8,128)(2,1)S(1)} %collective-permute-done.1), channel_id=1, source_target_pairs={{0,4},{4,8},{8,12},{12,0},{1,5},{5,9},{9,13},{13,1},{2,6},{6,10},{... | collective-permute-start | bytes 2433032 | tf_op jit(solution)/shard_map/ppermute | solution.py:78
  168.4 1.4 fusion.9
  169.8 2.7 fusion.17
  172.5 10.9 %collective-permute-done.2 = bf16[1056,384]{1,0:T(8,128)(2,1)S(1)} collective-permute-done((bf16[1056,384]{1,0:T(8,128)(2,1)S(1)}, bf16[1056,384]{1,0:T(8,128)(2,1)S(1)}, u32[]{:S(2)}, u32[]{:S(2)}) %collective-permute-start.2) | collective-permute-done | bytes 811040 | tf_op jit(solution)/shard_map/ppermute | solution.py:78
  183.4 1.1 constant_dynamic-update-slice_fusion.7
  184.4 1.1 constant_dynamic-update-slice_fusion.6
  190.7 1.1 constant_dynamic-update-slice_fusion
  191.8 3.0 %fusion.4 = f32[256,1056]{0,1:T(8,128)S(1)} fusion(bf16[1536,1056]{0,1:T(8,128)(2,1)} %all-gather.3.cloned.1.call-done, bf16[256,1536]{1,0:T(8,128)(2,1)S(1)} %copy-done.2, f32[1536]{0:T(1024)S(1)} %copy-done.10, f32[256]{0:T(256)S(1)} %add_rsqrt_fusion.1), kind=kOutput, calls=%fused_computation.6 | convolution fusion | flops 832585728 | bytes 5118976 | tf_op jit(solution)/shard_map/dot_general | solution.py:69
  195.4 6.5 %fusion.36 = f32[2,128,1056]{1,0,2:T(2,128)S(1)} fusion(f32[2,128,1056]{1,0,2:T(2,128)S(1)} %reshape.64, f32[1056]{0:T(1024)S(1)} %get-tuple-element.6, f32[1056]{0:T(1024)S(1)} %get-tuple-element.7, f32[1056]{0:T(1024)S(1)} %get-tuple-element.5), kind=kLoop, calls=%fused_computation.53 | loop fusion | flops 1351680 | bytes 2175360 | tf_op jit(solution)/shard_map/add | solution.py:18
  201.9 38.4 %all-gather.5.cloned.1.call-done = bf16[1536,1056]{0,1:T(8,128)(2,1)} async-done(((bf16[384,1056]{0,1:T(8,128)(2,1)}), bf16[1536,1056]{0,1:T(8,128)(2,1)}) %all-gather.5.cloned.1.call-update) | async-done | bytes 3244048 | tf_op jit(solution)/shard_map/all_gather | solution.py:65
  240.3 7.8 %fusion.6 = bf16[256,1536]{1,0:T(8,128)(2,1)} fusion(bf16[1056,3072]{1,0:T(8,128)(2,1)} %constant_dynamic-update-slice_fusion, s32[]{:T(128)S(6)} %select_n.14, bf16[1536,1056]{0,1:T(8,128)(2,1)} %all-gather.5.cloned.1.call-done, f32[132,8,2,128]{3,2,1,0:T(2,128)S(1)} %bitcast.30, f32[1056]{0:T(1024)S(1)} %copy-done.11, bf16[256,1536]{1,0:T(8,128)(2,1)S(1)} %copy-done.2, ...), kind=kOutput, calls=%fused_computation.8 | convolution fusion | flops 1666424832 | bytes 9153668 | tf_op jit(solution)/shard_map/dot_general | solution.py:82
  248.2 33.8 %all-reduce.7.cloned.1.call-done = bf16[256,1536]{1,0:T(8,128)(2,1)} async-done(((bf16[256,1536]{1,0:T(8,128)(2,1)}), bf16[256,1536]{1,0:T(8,128)(2,1)}) %all-reduce.7.cloned.1.call-update) | async-done | bytes 786448 | tf_op jit(solution)/shard_map/psum | solution.py:23
  282.0 1.4 fusion.11
  283.4 2.4 fusion.20
  (50 shorter events, 8.5 us)
Async XLA Ops:
  7.4 36.2 %copy-start.3 = (bf16[384,192]{0,1:T(8,128)(2,1)S(1)}, bf16[384,192]{0,1:T(8,128)(2,1)}, u32[]{:S(2)}) copy-start(bf16[384,192]{0,1:T(8,128)(2,1)} %param.18) | copy-start | bytes 442372
  7.4 52.2 %copy-start.1 = (bf16[256,1536]{1,0:T(8,128)(2,1)S(1)}, bf16[256,1536]{1,0:T(8,128)(2,1)}, u32[]{:S(2)}) copy-start(bf16[256,1536]{1,0:T(8,128)(2,1)} %param.15) | copy-start | bytes 2359300
  7.4 52.4 %copy-start.4 = (bf16[384,192]{0,1:T(8,128)(2,1)S(1)}, bf16[384,192]{0,1:T(8,128)(2,1)}, u32[]{:S(2)}) copy-start(bf16[384,192]{0,1:T(8,128)(2,1)} %param.19) | copy-start | bytes 442372
  7.4 161.0 %all-reduce.5.cloned.1.call-start = ((), (), s32[]{:S(2)}) async-start(), calls=%async_computation | async-start | bytes 1572864 | tf_op jit(solution)/shard_map/psum | solution.py:23
  26.2 49.7 %copy-start.9 = (f32[1536]{0:T(1024)S(1)}, f32[1536]{0:T(1024)}, u32[]{:S(2)}) copy-start(f32[1536]{0:T(1024)} %param.16) | copy-start | bytes 18436
  76.5 0.7 copy-start.8
  80.5 1.1 copy-start
  80.5 34.7 %copy-start.5 = (f32[3,1056]{1,0:T(4,128)S(1)}, f32[3,1056]{1,0:T(4,128)}, u32[]{:S(2)}) copy-start(f32[3,1056]{1,0:T(4,128)} %param.26) | copy-start | bytes 38020
  80.5 89.3 %copy-start.6 = (f32[1536]{0:T(1024)S(1)}, f32[1536]{0:T(1024)}, u32[]{:S(2)}) copy-start(f32[1536]{0:T(1024)} %param.22) | copy-start | bytes 18436
  80.5 111.3 %all-gather.3.cloned.1.call-start = ((), (), s32[]{:S(2)}) async-start(), calls=%async_computation.1 | async-start | bytes 4055040 | tf_op jit(solution)/shard_map/all_gather | solution.py:66
  81.1 159.3 %all-gather.5.cloned.1.call-start = ((), (), s32[]{:S(2)}) async-start(), calls=%async_computation.2 | async-start | bytes 4055040 | tf_op jit(solution)/shard_map/all_gather | solution.py:65
  81.6 28.1 %collective-permute-start = (bf16[1056,384]{1,0:T(8,128)(2,1)S(1)}, bf16[1056,384]{1,0:T(8,128)(2,1)S(1)}, u32[]{:S(2)}, u32[]{:S(2)}) collective-permute-start(bf16[1056,384]{1,0:T(8,128)(2,1)S(1)} %copy-done), channel_id=1, source_target_pairs={{0,4},{4,8},{8,12},{12,0},{1,5},{5,9},{9,13},{13,1},{2,6},{6,10},{... | collective-permute-start | bytes 2433032 | tf_op jit(solution)/shard_map/ppermute | solution.py:78
  90.0 191.9 %all-reduce.7.cloned.1.call-start = ((), (), s32[]{:S(2)}) async-start(), calls=%async_computation.3 | async-start | bytes 1572864 | tf_op jit(solution)/shard_map/psum | solution.py:23
  109.7 41.6 %collective-permute-start.1 = (bf16[1056,384]{1,0:T(8,128)(2,1)S(1)}, bf16[1056,384]{1,0:T(8,128)(2,1)S(1)}, u32[]{:S(2)}, u32[]{:S(2)}) collective-permute-start(bf16[1056,384]{1,0:T(8,128)(2,1)S(1)} %collective-permute-done), channel_id=1, source_target_pairs={{0,4},{4,8},{8,12},{12,0},{1,5},{5,9},{9,13},{13,1},{2,6},{6,10},{... | collective-permute-start | bytes 2433032 | tf_op jit(solution)/shard_map/ppermute | solution.py:78
  151.3 32.1 %collective-permute-start.2 = (bf16[1056,384]{1,0:T(8,128)(2,1)S(1)}, bf16[1056,384]{1,0:T(8,128)(2,1)S(1)}, u32[]{:S(2)}, u32[]{:S(2)}) collective-permute-start(bf16[1056,384]{1,0:T(8,128)(2,1)S(1)} %collective-permute-done.1), channel_id=1, source_target_pairs={{0,4},{4,8},{8,12},{12,0},{1,5},{5,9},{9,13},{13,1},{2,6},{6,10},{... | collective-permute-start | bytes 2433032 | tf_op jit(solution)/shard_map/ppermute | solution.py:78
  189.7 2.1 copy-start.2
  189.7 2.1 copy-start.10
  195.4 44.9 %copy-start.11 = (f32[1056]{0:T(1024)S(1)}, f32[1056]{0:T(1024)}, u32[]{:S(2)}) copy-start(f32[1056]{0:T(1024)} %param.27) | copy-start | bytes 12676
  248.2 35.2 %copy-start.7 = (f32[1536]{0:T(1024)S(1)}, f32[1536]{0:T(1024)}, u32[]{:S(2)}) copy-start(f32[1536]{0:T(1024)} %param.29) | copy-start | bytes 18436
Sparse Core Ops, SparseCore 0:
  80.6 40.8 all-reduce.4
  248.3 33.6 all-reduce.6
Sparse Core Ops, SparseCore 1:
  82.6 93.2 all-gather.2
  177.3 63.0 all-gather.4
